TPU v7x, 32 devices: a whole 2x2x4 slice. The times are simulated.
32 devices in a mesh: sp: 8 (over z, x), tp: 4 (over y, core).
Axes of the slice: x: 2, y: 2, z: 4, core: 2. Of those that a mesh axis runs over, the one named last changes fastest.
Arguments:
- queries: bfloat16 [1024, 2048], P('sp', 'tp'), may hold values from -6 to 6
- keys: bfloat16 [1024, 512], P('sp', 'tp'), may hold values from -6 to 6
- values: bfloat16 [1024, 512], P('sp', 'tp'), may hold values from -6 to 6
- break_bias: float32 [16], P('tp'), as said below
- residual: bfloat16 [1024, 4096], P(('sp', 'tp')), may hold values from -6 to 6
- w_out: bfloat16 [2048, 4096], P('tp'), may hold values from -0.125 to 0.125
- ffn_gain: float32 [4096], replicated, may hold values from 0.1 to 1.9
- pick_ids: int32 [1024, 2], P('sp'), may hold values from 0 to 7, as said below
- pair_logit: float32 [1024], P('sp'), may hold values from -8 to 8
- w_gate: bfloat16 [8, 4096, 1024], P('sp', None, 'tp'), may hold values from -0.09375 to 0.09375
- w_up: bfloat16 [8, 4096, 1024], P('sp', None, 'tp'), may hold values from -0.09375 to 0.09375
- w_down: bfloat16 [8, 1024, 4096], P('sp', 'tp'), may hold values from -0.1875 to 0.1875
- out_gain: float32 [4096], replicated, may hold values from 0.1 to 1.9
Outputs:
- new_stream: bfloat16 [1024, 4096], P(('sp', 'tp'))
Inputs may be any that keep to these rules, and one draw needn't show every extreme that they name: `break_bias`: the logarithm of a break rate per position: between ln(0.02 / 1024) and ln(8 / 128). `pick_ids`: A row's 2 experts differ and lie in one group of 2 consecutive experts. In each aligned block of 32 rows no expert is named more than 12 times, and some expert exactly 12 times.
All inputs are finite; a program needn't handle non-finite values.
Results may differ from a plain program's by a relative error of at most 0.017.
Values may be sent and summed in bfloat16 or wider, within the bound.
A program may use at most 64 MiB of HBM per device.

v0:
```python
import jax
import jax.numpy as jnp
from jax import lax
from jax.sharding import PartitionSpec as P

HEAD = 128
TOP = 2


epsilon = 1e-06


def passed_along(block, axis, distance):
    devices = range(lax.axis_size(axis))
    route = [(i - distance, i) for i in devices if i - distance in devices]
    return lax.ppermute(block, axis, route)


def stick_block(carried, query_rows, key_block, value_block, head_bias, query_pos, key_pos, usable):
    output, used_up = carried
    scores = jnp.einsum("qcgd,scd->qcgs", query_rows, key_block, preferred_element_type=jnp.float32)
    scores = scores * query_rows.shape[-1] ** (-0.5) + head_bias[None, :, :, None]
    before = ((key_pos[None, :] < query_pos[:, None]) & usable)[:, None, None, :]
    breaks = jnp.where(before, jax.nn.softplus(scores), 0.0)
    behind = lax.cumsum(breaks, axis=3, reverse=True) - breaks
    weights = jnp.where(
        before, jnp.exp(jax.nn.log_sigmoid(scores) - behind - used_up[..., None]), 0.0
    )
    output = output + jnp.einsum(
        "qcgs,scd->qcgd",
        weights.astype(jnp.bfloat16),
        value_block,
        preferred_element_type=jnp.float32,
    )
    return (output, used_up + jnp.sum(breaks, axis=3))


def normed_heads(output):
    scaled = output * lax.rsqrt(jnp.mean(output * output, axis=-1, keepdims=True) + epsilon)
    return scaled.astype(jnp.bfloat16).reshape(output.shape[0], -1)


def on_device(
    queries,
    keys,
    values,
    break_bias,
    residual,
    w_out,
    ffn_gain,
    pick_ids,
    pair_logit,
    w_gate,
    w_up,
    w_down,
    out_gain,
):
    length = queries.shape[0]
    kv_local = keys.shape[1] // HEAD
    per_key = queries.shape[1] // keys.shape[1]
    query_rows = queries.reshape(length, kv_local, per_key, HEAD)
    head_bias = break_bias.reshape(kv_local, per_key)
    position = lax.axis_index("sp")
    offset = position * length
    query_pos = offset + jnp.arange(length, dtype=jnp.int32)
    initial = (
        jnp.zeros((length, kv_local, per_key, HEAD), jnp.float32),
        jnp.zeros((length, kv_local, per_key), jnp.float32),
    )
    stacked = jnp.stack([keys, values])
    carried = stick_block(
        initial,
        query_rows,
        keys.reshape(length, kv_local, HEAD),
        values.reshape(length, kv_local, HEAD),
        head_bias,
        query_pos,
        query_pos,
        True,
    )

    def visit(step_index, loop_state):
        arrived_pair, carried = loop_state
        arrived_pair = passed_along(arrived_pair, "sp", 1)
        source = position - step_index
        key_pos = source * length + jnp.arange(length, dtype=jnp.int32)
        carried = stick_block(
            carried,
            query_rows,
            arrived_pair[0].reshape(length, kv_local, HEAD),
            arrived_pair[1].reshape(length, kv_local, HEAD),
            head_bias,
            query_pos,
            key_pos,
            source >= 0,
        )
        return (arrived_pair, carried)

    head_out = normed_heads(lax.fori_loop(1, lax.axis_size("sp"), visit, (stacked, carried))[1][0])
    quarters = lax.axis_size("tp")
    quarter = lax.axis_index("tp")
    slice_rows = length // quarters
    width = w_out.shape[1]
    experts = lax.axis_size("sp")
    capacity = max(2, (3 * slice_rows + experts - 1) // experts)
    mixed = lax.psum_scatter(
        jnp.dot(head_out, w_out, preferred_element_type=jnp.float32).astype(jnp.bfloat16),
        "tp",
        scatter_dimension=0,
        tiled=True,
    ).astype(jnp.float32)
    stream = (residual.astype(jnp.float32) + mixed).astype(jnp.bfloat16)
    routed = lax.dynamic_slice_in_dim(pick_ids, quarter * slice_rows, slice_rows, 0)[None]
    stream_float = stream.astype(jnp.float32)
    ffn_in = (
        stream_float
        * lax.rsqrt(jnp.mean(stream_float * stream_float, axis=-1, keepdims=True) + epsilon)
        * ffn_gain
    ).astype(jnp.bfloat16)
    blocks = routed.shape[0]
    entries = ffn_in.reshape(blocks, slice_rows, width)
    flat_ids = routed.reshape(blocks, slice_rows * TOP)
    places = jnp.arange(slice_rows * TOP, dtype=jnp.int32)
    earlier = places[None, :] < places[:, None]
    matches = (flat_ids[:, :, None] == flat_ids[:, None, :]) & earlier[None]
    ranks = jnp.sum(matches.astype(jnp.int32), axis=2)
    targets = (flat_ids * capacity + ranks).reshape(blocks, slice_rows, TOP)
    block_ids = jnp.arange(blocks, dtype=jnp.int32)[:, None]
    outgoing = jnp.zeros((blocks, experts * capacity, width), jnp.bfloat16)
    for pick_index in range(TOP):
        outgoing = outgoing.at[block_ids, targets[:, :, pick_index]].set(entries)
    arrived = lax.all_to_all(outgoing, "sp", split_axis=1, concat_axis=1, tiled=True).reshape(
        -1, width
    )
    piece = lax.all_gather(arrived, "tp", axis=0, tiled=True)
    gated = jax.nn.silu(jnp.dot(piece, w_gate[0], preferred_element_type=jnp.float32))
    hidden = (gated * jnp.dot(piece, w_up[0], preferred_element_type=jnp.float32)).astype(
        jnp.bfloat16
    )
    results = lax.psum_scatter(
        jnp.dot(hidden, w_down[0], preferred_element_type=jnp.float32).astype(jnp.bfloat16),
        "tp",
        scatter_dimension=0,
        tiled=True,
    )
    returned = lax.all_to_all(results, "sp", split_axis=0, concat_axis=0, tiled=True)
    own_targets = targets[0]
    logits = lax.dynamic_slice_in_dim(pair_logit, quarter * slice_rows, slice_rows, 0)
    leading = returned[own_targets[:, 0]].astype(jnp.float32)
    trailing = returned[own_targets[:, 1]].astype(jnp.float32)
    blended = (
        jax.nn.sigmoid(logits)[:, None] * leading + jax.nn.sigmoid(-logits)[:, None] * trailing
    )
    blend_scale = lax.rsqrt(jnp.mean(blended * blended, axis=-1, keepdims=True) + epsilon)
    return (stream_float + blended * blend_scale * out_gain).astype(jnp.bfloat16)


def solution(mesh):
    placed = (
        P("sp", "tp"),
        P("sp", "tp"),
        P("sp", "tp"),
        P("tp"),
        P(("sp", "tp"), None),
        P("tp", None),
        P(),
        P("sp", None),
        P("sp"),
        P("sp", None, "tp"),
        P("sp", None, "tp"),
        P("sp", "tp", None),
        P(),
    )
    return jax.shard_map(
        on_device, mesh=mesh, in_specs=placed, out_specs=P(("sp", "tp"), None), check_vma=False
    )
```

profile of v0, /device:TPU:0, one launch (start us, length us, event | category | flops | bytes accessed | tf_op | source)
XLA Modules:
  0.0 276.8 jit_solution(1136986469250857039)
XLA Ops:
  6.7 1.1 copy.84
  8.0 1.3 fusion.82
  9.2 1.2 fusion.64
  10.4 0.6 convolution_bitcast_fusion.1
  11.0 62.2 %while.18 = (s32[]{:T(128)}, bf16[2,128,128]{2,1,0:T(8,128)(2,1)S(1)}, f32[128,1,4,128]{3,0,2,1:T(8,128)S(1)}, f32[128,1,4]{0,2,1:T(4,128)S(1)}, s32[]{:T(128)},...) while((s32[]{:T(128)}, ...), condition=%wide.region_5.6_spmd.clone, body=%wide.region_2.5_spmd.clone.sunk | while | flops 43942148 | bytes 2749119 | solution.py:99
  11.0 4.9 %collective-permute-start = (bf16[2,128,128]{2,1,0:T(8,128)(2,1)S(1)}, bf16[2,128,128]{2,1,0:T(8,128)(2,1)S(1)}, u32[]{:S(2)}, u32[]{:S(2)}) collective-permute-start(bf16[2,128,128]{2,1,0:T(8,128)(2,1)S(1)} %get-tuple-element.307), channel_id=1, source_target_pairs={{0,4},{4,8},{8,12},{12,16},{16,20},{20,24},{24,28},{1,5},{5,9},{9,... | collective-permute-start | bytes 196616 | tf_op jit(solution)/shard_map/while/body/eval_jaxpr/ppermute | solution.py:16
  16.0 1.8 collective-permute-done
  17.8 0.3 fusion.96
  18.1 1.2 fusion.97
  19.3 0.6 fusion.98
  19.9 4.3 %collective-permute-start = (bf16[2,128,128]{2,1,0:T(8,128)(2,1)S(1)}, bf16[2,128,128]{2,1,0:T(8,128)(2,1)S(1)}, u32[]{:S(2)}, u32[]{:S(2)}) collective-permute-start(bf16[2,128,128]{2,1,0:T(8,128)(2,1)S(1)} %get-tuple-element.307), channel_id=1, source_target_pairs={{0,4},{4,8},{8,12},{12,16},{16,20},{20,24},{24,28},{1,5},{5,9},{9,... | collective-permute-start | bytes 196616 | tf_op jit(solution)/shard_map/while/body/eval_jaxpr/ppermute | solution.py:16
  24.3 1.8 collective-permute-done
  26.0 0.3 fusion.96
  26.4 1.2 fusion.97
  27.6 0.6 fusion.98
  28.2 4.4 %collective-permute-start = (bf16[2,128,128]{2,1,0:T(8,128)(2,1)S(1)}, bf16[2,128,128]{2,1,0:T(8,128)(2,1)S(1)}, u32[]{:S(2)}, u32[]{:S(2)}) collective-permute-start(bf16[2,128,128]{2,1,0:T(8,128)(2,1)S(1)} %get-tuple-element.307), channel_id=1, source_target_pairs={{0,4},{4,8},{8,12},{12,16},{16,20},{20,24},{24,28},{1,5},{5,9},{9,... | collective-permute-start | bytes 196616 | tf_op jit(solution)/shard_map/while/body/eval_jaxpr/ppermute | solution.py:16
  32.6 1.8 collective-permute-done
  34.4 0.3 fusion.96
  34.8 1.2 fusion.97
  35.9 0.6 fusion.98
  36.5 5.2 %collective-permute-start = (bf16[2,128,128]{2,1,0:T(8,128)(2,1)S(1)}, bf16[2,128,128]{2,1,0:T(8,128)(2,1)S(1)}, u32[]{:S(2)}, u32[]{:S(2)}) collective-permute-start(bf16[2,128,128]{2,1,0:T(8,128)(2,1)S(1)} %get-tuple-element.307), channel_id=1, source_target_pairs={{0,4},{4,8},{8,12},{12,16},{16,20},{20,24},{24,28},{1,5},{5,9},{9,... | collective-permute-start | bytes 196616 | tf_op jit(solution)/shard_map/while/body/eval_jaxpr/ppermute | solution.py:16
  41.8 1.8 collective-permute-done
  43.6 0.3 fusion.96
  44.0 1.2 fusion.97
  45.1 0.6 fusion.98
  45.7 5.2 %collective-permute-start = (bf16[2,128,128]{2,1,0:T(8,128)(2,1)S(1)}, bf16[2,128,128]{2,1,0:T(8,128)(2,1)S(1)}, u32[]{:S(2)}, u32[]{:S(2)}) collective-permute-start(bf16[2,128,128]{2,1,0:T(8,128)(2,1)S(1)} %get-tuple-element.307), channel_id=1, source_target_pairs={{0,4},{4,8},{8,12},{12,16},{16,20},{20,24},{24,28},{1,5},{5,9},{9,... | collective-permute-start | bytes 196616 | tf_op jit(solution)/shard_map/while/body/eval_jaxpr/ppermute | solution.py:16
  51.0 1.8 collective-permute-done
  52.8 0.3 fusion.96
  53.1 1.2 fusion.97
  54.3 0.6 fusion.98
  54.9 5.2 %collective-permute-start = (bf16[2,128,128]{2,1,0:T(8,128)(2,1)S(1)}, bf16[2,128,128]{2,1,0:T(8,128)(2,1)S(1)}, u32[]{:S(2)}, u32[]{:S(2)}) collective-permute-start(bf16[2,128,128]{2,1,0:T(8,128)(2,1)S(1)} %get-tuple-element.307), channel_id=1, source_target_pairs={{0,4},{4,8},{8,12},{12,16},{16,20},{20,24},{24,28},{1,5},{5,9},{9,... | collective-permute-start | bytes 196616 | tf_op jit(solution)/shard_map/while/body/eval_jaxpr/ppermute | solution.py:16
  60.2 1.8 collective-permute-done
  62.0 0.3 fusion.96
  62.3 1.2 fusion.97
  63.5 0.6 fusion.98
  64.1 5.2 %collective-permute-start = (bf16[2,128,128]{2,1,0:T(8,128)(2,1)S(1)}, bf16[2,128,128]{2,1,0:T(8,128)(2,1)S(1)}, u32[]{:S(2)}, u32[]{:S(2)}) collective-permute-start(bf16[2,128,128]{2,1,0:T(8,128)(2,1)S(1)} %get-tuple-element.307), channel_id=1, source_target_pairs={{0,4},{4,8},{8,12},{12,16},{16,20},{20,24},{24,28},{1,5},{5,9},{9,... | collective-permute-start | bytes 196616 | tf_op jit(solution)/shard_map/while/body/eval_jaxpr/ppermute | solution.py:16
  69.4 1.8 collective-permute-done
  71.1 0.4 fusion.96
  71.5 1.1 fusion.97
  72.6 0.6 fusion.98
  73.6 4.0 %convolution_convert_fusion.1 = bf16[128,4096]{1,0:T(8,128)(2,1)} fusion(bf16[128,512]{0,1:T(8,128)(2,1)S(1)} %bitcast.134, bf16[512,4096]{1,0:T(8,128)(2,1)} %param.20), kind=kOutput, calls=%fused_computation.36 | convolution fusion | flops 537395200 | bytes 5373952 | tf_op jit(solution)/shard_map/dot_general | solution.py:107
  78.9 27.4 %reduce-scatter.3.cloned.1.call-done = bf16[32,4096]{1,0:T(8,128)(2,1)} async-done(((bf16[128,4096]{1,0:T(8,128)(2,1)}), bf16[32,4096]{1,0:T(8,128)(2,1)}) %reduce-scatter.3.cloned.1.call-update) | async-done | bytes 262160 | tf_op jit(solution)/shard_map/reduce_scatter | solution.py:106
  106.4 1.2 fusion.47
  107.6 1.3 scatter_custom_fusion
  108.9 1.7 scatter_custom_fusion.1
  110.6 2.9 %copy.126 = bf16[1,96,4096]{2,0,1:T(2,128)(2,1)} copy(bf16[1,96,4096]{2,1,0:T(8,128)(2,1)S(1)} %bitcast.132) | data formatting | bytes 1572864 | tf_op jit(solution)/shard_map/scatter | solution.py:131
  113.5 0.5 broadcast.261
  114.0 6.7 %reduce.14 = bf16[96,4096]{1,0:T(8,128)(2,1)S(1)} reduce(bf16[96,1,4096]{2,1,0:T(2,128)(2,1)} %bitcast.130, bf16[]{:T(256)} %broadcast.261), dimensions={1}, to_apply=%bitcast.113.reduce_sub_computation | reduce | bytes 1572866
  120.7 1.6 reshape.361
  122.3 25.5 %all_to_all.17 = bf16[8,2,24576]{2,1,0:T(2,128)(2,1)S(1)} all-to-all(bf16[8,2,24576]{2,1,0:T(2,128)(2,1)} %reshape.361), channel_id=1, replica_groups=mesh['sp'=8,'tp'=4] {'sp'}, dimensions={0} | all-to-all | bytes 1572864 | tf_op jit(solution)/shard_map/all_to_all | solution.py:132
  147.8 3.2 %reshape.362 = bf16[96,1,4096]{2,1,0:T(2,128)(2,1)} reshape(bf16[8,2,24576]{2,1,0:T(2,128)(2,1)S(1)} %all_to_all.17) | data formatting | bytes 1572864
  150.9 3.1 %copy.94 = bf16[1,96,4096]{2,1,0:T(8,128)(2,1)} copy(bf16[1,96,4096]{2,0,1:T(2,128)(2,1)} %bitcast.131) | data formatting | bytes 1572864 | tf_op jit(solution)/shard_map/all_to_all | solution.py:132
  154.2 26.7 %all-gather.3.cloned.1.call-done = bf16[1,384,4096]{2,1,0:T(8,128)(2,1)} async-done(((bf16[1,96,4096]{2,1,0:T(8,128)(2,1)}), bf16[1,384,4096]{2,1,0:T(8,128)(2,1)}) %all-gather.3.cloned.1.call-update) | async-done | bytes 3145744 | tf_op jit(solution)/shard_map/all_gather | solution.py:135
  180.9 3.5 %fusion.25 = f32[384,256]{1,0:T(8,128)S(1)} fusion(bf16[1,384,4096]{2,1,0:T(8,128)(2,1)} %all-gather.3.cloned.1.call-done, bf16[1,4096,256]{2,1,0:T(8,128)(2,1)} %param.24), kind=kOutput, calls=%fused_computation.39 | convolution fusion | flops 805306368 | bytes 5636096 | tf_op jit(solution)/shard_map/dot_general | solution.py:136
  184.4 7.7 %convolution_convert_fusion = bf16[384,4096]{1,0:T(8,128)(2,1)} fusion(bf16[1,256,4096]{2,1,0:T(8,128)(2,1)S(1)} %copy-done, bf16[1,4096,256]{2,1,0:T(8,128)(2,1)} %param.25, bf16[1,384,4096]{2,1,0:T(8,128)(2,1)} %all-gather.3.cloned.1.call-done, f32[384,256]{1,0:T(8,128)S(1)} %fusion.25), kind=kOutput, calls=%fused_computation.35 | convolution fusion | flops 1612775424 | bytes 10878976 | tf_op jit(solution)/shard_map/dot_general | solution.py:141
  192.1 38.0 %reduce-scatter.5.cloned.1.call-done = bf16[96,4096]{1,0:T(8,128)(2,1)} async-done(((bf16[384,4096]{1,0:T(8,128)(2,1)}), bf16[96,4096]{1,0:T(8,128)(2,1)}) %reduce-scatter.5.cloned.1.call-update) | async-done | bytes 786448 | tf_op jit(solution)/shard_map/reduce_scatter | solution.py:140
  230.2 2.2 all_to_all.12
  232.3 5.5 %all-to-all-start.1 = ((bf16[8,12,4096]{2,1,0:T(8,128)(2,1)}), bf16[8,12,4096]{2,1,0:T(8,128)(2,1)}, u32[]{:S(2)}, u32[]{:S(2)}) async-start(bf16[8,12,4096]{2,1,0:T(8,128)(2,1)} %all_to_all.12), calls=%async_computation.3 | async-start | bytes 2097152 | tf_op jit(solution)/shard_map/all_to_all | solution.py:146
  238.1 25.5 %all-to-all-done.1 = bf16[8,12,4096]{2,1,0:T(8,128)(2,1)} async-done(((bf16[8,12,4096]{2,1,0:T(8,128)(2,1)}), bf16[8,12,4096]{2,1,0:T(8,128)(2,1)}, u32[]{:S(2)}, u32[]{:S(2)}) %all-to-all-start.1) | async-done | bytes 786464 | tf_op jit(solution)/shard_map/all_to_all | solution.py:146
  263.6 1.4 all_to_all.14
  265.0 0.7 gather_fusion.1
  265.7 1.4 gather_fusion
  267.1 1.2 multiply_reduce_fusion
  268.4 1.9 fusion.50
  (82 shorter events, 3.0 us)
Async XLA Ops:
  6.5 177.9 %copy-start = (bf16[1,256,4096]{2,1,0:T(8,128)(2,1)S(1)}, bf16[1,256,4096]{2,1,0:T(8,128)(2,1)}, u32[]{:S(2)}) copy-start(bf16[1,256,4096]{2,1,0:T(8,128)(2,1)} %param.26) | copy-start | bytes 6291460
  6.5 4.5 %copy-start.8 = (f32[4]{0:T(128)S(1)}, f32[4]{0:T(128)}, u32[]{:S(2)}) copy-start(f32[4]{0:T(128)} %param.18) | copy-start | bytes 52
  6.5 3.9 %copy-start.3 = (bf16[128,128]{1,0:T(8,128)(2,1)S(1)}, bf16[128,128]{1,0:T(8,128)(2,1)}, u32[]{:S(2)}) copy-start(bf16[128,128]{1,0:T(8,128)(2,1)} %param.16) | copy-start | bytes 98308
  6.5 3.9 %copy-start.4 = (bf16[128,128]{1,0:T(8,128)(2,1)S(1)}, bf16[128,128]{1,0:T(8,128)(2,1)}, u32[]{:S(2)}) copy-start(bf16[128,128]{1,0:T(8,128)(2,1)} %param.17) | copy-start | bytes 98308
  6.5 99.8 %reduce-scatter.3.cloned.1.call-start = ((), (), s32[]{:S(2)}) async-start(), calls=%async_computation.4 | async-start | bytes 1310720 | tf_op jit(solution)/shard_map/reduce_scatter | solution.py:106
  11.0 6.8 %collective-permute-start = (bf16[2,128,128]{2,1,0:T(8,128)(2,1)S(1)}, bf16[2,128,128]{2,1,0:T(8,128)(2,1)S(1)}, u32[]{:S(2)}, u32[]{:S(2)}) collective-permute-start(bf16[2,128,128]{2,1,0:T(8,128)(2,1)S(1)} %get-tuple-element.307), channel_id=1, source_target_pairs={{0,4},{4,8},{8,12},{12,16},{16,20},{20,24},{24,28},{1,5},{5,9},{9,... | collective-permute-start | bytes 196616 | tf_op jit(solution)/shard_map/while/body/eval_jaxpr/ppermute | solution.py:16
  19.9 6.2 %collective-permute-start = (bf16[2,128,128]{2,1,0:T(8,128)(2,1)S(1)}, bf16[2,128,128]{2,1,0:T(8,128)(2,1)S(1)}, u32[]{:S(2)}, u32[]{:S(2)}) collective-permute-start(bf16[2,128,128]{2,1,0:T(8,128)(2,1)S(1)} %get-tuple-element.307), channel_id=1, source_target_pairs={{0,4},{4,8},{8,12},{12,16},{16,20},{20,24},{24,28},{1,5},{5,9},{9,... | collective-permute-start | bytes 196616 | tf_op jit(solution)/shard_map/while/body/eval_jaxpr/ppermute | solution.py:16
  28.2 6.2 %collective-permute-start = (bf16[2,128,128]{2,1,0:T(8,128)(2,1)S(1)}, bf16[2,128,128]{2,1,0:T(8,128)(2,1)S(1)}, u32[]{:S(2)}, u32[]{:S(2)}) collective-permute-start(bf16[2,128,128]{2,1,0:T(8,128)(2,1)S(1)} %get-tuple-element.307), channel_id=1, source_target_pairs={{0,4},{4,8},{8,12},{12,16},{16,20},{20,24},{24,28},{1,5},{5,9},{9,... | collective-permute-start | bytes 196616 | tf_op jit(solution)/shard_map/while/body/eval_jaxpr/ppermute | solution.py:16
  36.5 7.1 %collective-permute-start = (bf16[2,128,128]{2,1,0:T(8,128)(2,1)S(1)}, bf16[2,128,128]{2,1,0:T(8,128)(2,1)S(1)}, u32[]{:S(2)}, u32[]{:S(2)}) collective-permute-start(bf16[2,128,128]{2,1,0:T(8,128)(2,1)S(1)} %get-tuple-element.307), channel_id=1, source_target_pairs={{0,4},{4,8},{8,12},{12,16},{16,20},{20,24},{24,28},{1,5},{5,9},{9,... | collective-permute-start | bytes 196616 | tf_op jit(solution)/shard_map/while/body/eval_jaxpr/ppermute | solution.py:16
  45.7 7.1 %collective-permute-start = (bf16[2,128,128]{2,1,0:T(8,128)(2,1)S(1)}, bf16[2,128,128]{2,1,0:T(8,128)(2,1)S(1)}, u32[]{:S(2)}, u32[]{:S(2)}) collective-permute-start(bf16[2,128,128]{2,1,0:T(8,128)(2,1)S(1)} %get-tuple-element.307), channel_id=1, source_target_pairs={{0,4},{4,8},{8,12},{12,16},{16,20},{20,24},{24,28},{1,5},{5,9},{9,... | collective-permute-start | bytes 196616 | tf_op jit(solution)/shard_map/while/body/eval_jaxpr/ppermute | solution.py:16
  54.9 7.1 %collective-permute-start = (bf16[2,128,128]{2,1,0:T(8,128)(2,1)S(1)}, bf16[2,128,128]{2,1,0:T(8,128)(2,1)S(1)}, u32[]{:S(2)}, u32[]{:S(2)}) collective-permute-start(bf16[2,128,128]{2,1,0:T(8,128)(2,1)S(1)} %get-tuple-element.307), channel_id=1, source_target_pairs={{0,4},{4,8},{8,12},{12,16},{16,20},{20,24},{24,28},{1,5},{5,9},{9,... | collective-permute-start | bytes 196616 | tf_op jit(solution)/shard_map/while/body/eval_jaxpr/ppermute | solution.py:16
  64.1 7.1 %collective-permute-start = (bf16[2,128,128]{2,1,0:T(8,128)(2,1)S(1)}, bf16[2,128,128]{2,1,0:T(8,128)(2,1)S(1)}, u32[]{:S(2)}, u32[]{:S(2)}) collective-permute-start(bf16[2,128,128]{2,1,0:T(8,128)(2,1)S(1)} %get-tuple-element.307), channel_id=1, source_target_pairs={{0,4},{4,8},{8,12},{12,16},{16,20},{20,24},{24,28},{1,5},{5,9},{9,... | collective-permute-start | bytes 196616 | tf_op jit(solution)/shard_map/while/body/eval_jaxpr/ppermute | solution.py:16
  73.6 4.1 %copy-start.6 = (s32[128,2]{0,1:T(2,128)S(1)}, s32[128,2]{0,1:T(2,128)}, u32[]{:S(2)}) copy-start(s32[128,2]{0,1:T(2,128)} %param.22) | copy-start | bytes 3076
  73.6 32.8 %copy-start.1 = (bf16[32,4096]{1,0:T(8,128)(2,1)S(1)}, bf16[32,4096]{1,0:T(8,128)(2,1)}, u32[]{:S(2)}) copy-start(bf16[32,4096]{1,0:T(8,128)(2,1)} %param.19) | copy-start | bytes 786436
  77.6 30.0 %copy-start.2 = (f32[4096]{0:T(1024)S(1)}, f32[4096]{0:T(1024)}, u32[]{:S(2)}) copy-start(f32[4096]{0:T(1024)} %param.21) | copy-start | bytes 49156
  77.6 103.3 %all-gather.3.cloned.1.call-start = ((), (), s32[]{:S(2)}) async-start(), calls=%async_computation.6 | async-start | bytes 3932160 | tf_op jit(solution)/shard_map/all_gather | solution.py:135
  154.1 76.0 %reduce-scatter.5.cloned.1.call-start = ((), (), s32[]{:S(2)}) async-start(), calls=%async_computation.5 | async-start | bytes 3932160 | tf_op jit(solution)/shard_map/reduce_scatter | solution.py:140
  192.1 45.8 %copy-start.7 = (f32[128]{0:T(128)S(1)}, f32[128]{0:T(128)}, u32[]{:S(2)}) copy-start(f32[128]{0:T(128)} %param.23) | copy-start | bytes 1540
  232.3 31.3 %all-to-all-start.1 = ((bf16[8,12,4096]{2,1,0:T(8,128)(2,1)}), bf16[8,12,4096]{2,1,0:T(8,128)(2,1)}, u32[]{:S(2)}, u32[]{:S(2)}) async-start(bf16[8,12,4096]{2,1,0:T(8,128)(2,1)} %all_to_all.12), calls=%async_computation.3 | async-start | bytes 2097152 | tf_op jit(solution)/shard_map/all_to_all | solution.py:146
  265.0 3.4 %copy-start.5 = (f32[4096]{0:T(1024)S(1)}, f32[4096]{0:T(1024)}, u32[]{:S(2)}) copy-start(f32[4096]{0:T(1024)} %param.27) | copy-start | bytes 49156
Sparse Core Ops, SparseCore 0:
  77.7 28.6 reduce-scatter.2
  154.2 26.5 all-gather.2
  192.2 37.8 reduce-scatter.4
where the time goes:
time: 277 us
  waiting for transfers between devices  130 us (47%)
  starting transfers between devices  39.8 us (14%)
  blocking collectives  25.5 us (9%)
  other arithmetic  24.8 us (9%)
  matrix products  23.4 us (8%)
  local copies, waits for them, and re-layouts  19.4 us (7%)
  between operations  13.4 us (5%)
    reduce_scatter x1, waiting for transfers between devices, on_device(): lax.psum_scatter(jnp.dot(hidden, w_down[0], preferred_element_type=jnp.fl...  38 us
    ppermute x7, starting transfers between devices, passed_along(): return lax.ppermute(block, axis, route)  34.2 us
    reduce_scatter x1, waiting for transfers between devices, on_device(): lax.psum_scatter(jnp.dot(head_out, w_out, preferred_element_type=jnp.floa...  27.4 us
    all_gather x1, waiting for transfers between devices, on_device(): piece = lax.all_gather(arrived, 'tp', axis=0, tiled=True)  26.7 us
    all_to_all x1, waiting for transfers between devices, on_device(): lax.all_to_all(results, 'sp', split_axis=0, concat_axis=0, tiled=True)  25.5 us
    all_to_all x1, blocking collectives, on_device(): lax.all_to_all(outgoing, 'sp', split_axis=1, concat_axis=1, tiled=True)  25.5 us
    ppermute x7, waiting for transfers between devices, passed_along(): return lax.ppermute(block, axis, route)  12.4 us
    another operation x8, other arithmetic, stick_block(): behind = lax.cumsum(breaks, axis=3, reverse=True) - breaks  9.21 us
  transfers between devices with their start and end apart: 11, of which 11 were waited for; matrix products, arithmetic and copies ran while one was open for 1% of the time, Pallas kernels for 0%

commit v1 on v0

v1 whole, which is shorter than its diff:
```python
import functools

import jax
import jax.numpy as jnp
from jax import lax
from jax.experimental import pallas as pl
from jax.experimental.pallas import tpu as pltpu
from jax.sharding import PartitionSpec as P

HEAD = 128
TOP = 2
MESH = pl.DeviceIdType.MESH
TILES = 4

epsilon = 1e-06


def attend_block(query, key_block, value_block, bias, acc, used, diagonal):
    rows = query.shape[0]
    length = key_block.shape[0]
    scores = lax.dot_general(
        query, key_block, (((1,), (1,)), ((), ())), preferred_element_type=jnp.float32
    )
    scores = scores * HEAD ** (-0.5) + bias
    breaks = jnp.maximum(scores, 0.0) + jnp.log1p(jnp.exp(-jnp.abs(scores)))
    stays = scores - breaks
    if diagonal:
        at_row = lax.broadcasted_iota(jnp.int32, (rows, length), 0) % length
        at_col = lax.broadcasted_iota(jnp.int32, (rows, length), 1)
        before = at_col < at_row
        breaks = jnp.where(before, breaks, 0.0)
    later = (
        lax.broadcasted_iota(jnp.int32, (length, length), 0)
        > lax.broadcasted_iota(jnp.int32, (length, length), 1)
    ).astype(jnp.bfloat16)
    coarse = breaks.astype(jnp.bfloat16)
    fine = (breaks - coarse.astype(jnp.float32)).astype(jnp.bfloat16)
    behind = jnp.dot(coarse, later, preferred_element_type=jnp.float32) + jnp.dot(
        fine, later, preferred_element_type=jnp.float32
    )
    weights = jnp.exp(stays - behind - used[...])
    if diagonal:
        weights = jnp.where(before, weights, 0.0)
    acc[...] += jnp.dot(
        weights.astype(jnp.bfloat16), value_block, preferred_element_type=jnp.float32
    )
    used[...] += behind[:, :1] + breaks[:, :1]


def attention_part(
    n_sp, n_tp, q_ref, k_ref, v_ref, bias_ref, w_ref, res_ref, gain_ref,
    stream_ref, ffn_ref, kv_buf, w_buf, accs, useds, parts, recvs,
    w_sem, kv_send, kv_relay, kv_recv, rs_send, rs_recv,
):
    me, mine = lax.axis_index("sp"), lax.axis_index("tp")
    length = q_ref.shape[0]
    kv_local = k_ref.shape[1] // HEAD
    per_key = q_ref.shape[1] // k_ref.shape[1]
    rows = length // n_tp
    width = w_buf.shape[1]
    cols = width // TILES
    load = pltpu.make_async_copy(w_ref, w_buf, w_sem)
    load.start()
    pair, side = me // 2, me % 2
    mate = me + 1 - 2 * side
    sources = (k_ref, v_ref)

    def direct(kind, target):
        return pltpu.make_async_remote_copy(
            src_ref=sources[kind], dst_ref=kv_buf.at[kind, me],
            send_sem=kv_send.at[kind, target], recv_sem=kv_recv.at[kind, me],
            device_id=(target, mine), device_id_type=MESH,
        )

    def relay(kind, source):
        return pltpu.make_async_remote_copy(
            src_ref=kv_buf.at[kind, source], dst_ref=kv_buf.at[kind, source],
            send_sem=kv_relay.at[kind, source], recv_sem=kv_recv.at[kind, source],
            device_id=(mate, mine), device_id_type=MESH,
        )

    for kind in range(2):
        direct(kind, mate).start()

    def send_on(other, carry):
        for kind in range(2):
            direct(kind, 2 * other + side).start()
        return carry

    lax.fori_loop(pair + 1, n_sp // 2, send_on, 0)

    queries, biases = [], []
    for c in range(kv_local):
        heads = [c * per_key + g for g in range(per_key)]
        queries.append(
            jnp.concatenate([q_ref[:, h * HEAD : (h + 1) * HEAD] for h in heads], axis=0)
        )
        biases.append(
            jnp.concatenate([jnp.full((length, 1), bias_ref[h], jnp.float32) for h in heads], axis=0)
        )
    accs[...] = jnp.zeros_like(accs)
    useds[...] = jnp.zeros_like(useds)
    for c in range(kv_local):
        at = slice(c * HEAD, (c + 1) * HEAD)
        attend_block(
            queries[c], k_ref[:, at], v_ref[:, at], biases[c], accs.at[c], useds.at[c], True
        )

    def visit(step, carry):
        source = me - step
        for kind in range(2):
            relay(kind, source).wait_recv()

        @pl.when(step % 2 == 0)
        def _():
            for kind in range(2):
                relay(kind, source).start()

        for c in range(kv_local):
            at = slice(c * HEAD, (c + 1) * HEAD)
            attend_block(
                queries[c], kv_buf[0, source][:, at], kv_buf[1, source][:, at],
                biases[c], accs.at[c], useds.at[c], False,
            )
        return carry

    lax.fori_loop(1, me + 1, visit, 0)

    @pl.when(side == 0)
    def _():
        for kind in range(2):
            relay(kind, mate).wait_recv()

    pieces = []
    for c in range(kv_local):
        out = accs[c]
        out = out * lax.rsqrt(jnp.mean(out * out, axis=-1, keepdims=True) + epsilon)
        out = out.astype(jnp.bfloat16)
        pieces += [out[g * length : (g + 1) * length] for g in range(per_key)]
    head_out = jnp.concatenate(pieces, axis=1)
    load.wait()

    levels = len(recvs)

    def share(level, tile, i):
        bit = (mine >> level) % 2
        at = pl.ds(tile * cols, cols)
        return pltpu.make_async_remote_copy(
            src_ref=parts[level].at[2 * i + 1 - bit, :, at],
            dst_ref=recvs[level].at[i, :, at],
            send_sem=rs_send.at[level, tile, i], recv_sem=rs_recv.at[level, tile, i],
            device_id=(me, mine + (1 - 2 * bit) * (1 << level)), device_id_type=MESH,
        )

    for tile in range(TILES):
        at = slice(tile * cols, (tile + 1) * cols)
        product = jnp.dot(head_out, w_buf[:, at], preferred_element_type=jnp.float32)
        parts[0][:, :, at] = product.astype(jnp.bfloat16).reshape(n_tp, rows, cols)
        for i in range(n_tp // 2):
            share(0, tile, i).start()
    squares = jnp.zeros((rows, 1), jnp.float32)
    for level in range(levels):
        bit = (mine >> level) % 2
        count = n_tp >> (level + 1)
        for tile in range(TILES):
            at = slice(tile * cols, (tile + 1) * cols)
            for i in range(count):
                share(level, tile, i).wait_recv()
                total = parts[level][2 * i + bit, :, at].astype(jnp.float32) + recvs[level][
                    i, :, at
                ].astype(jnp.float32)
                if level + 1 < levels:
                    parts[level + 1][i, :, at] = total.astype(jnp.bfloat16)
                else:
                    total = (total + res_ref[:, at].astype(jnp.float32)).astype(jnp.bfloat16)
                    stream_ref[:, at] = total
                    total = total.astype(jnp.float32)
                    squares += jnp.sum(total * total, axis=1, keepdims=True)
            if level + 1 < levels:
                for i in range(count // 2):
                    share(level + 1, tile, i).start()
    scale = lax.rsqrt(squares / width + epsilon)
    for tile in range(TILES):
        at = slice(tile * cols, (tile + 1) * cols)
        ffn_ref[:, at] = (
            stream_ref[:, at].astype(jnp.float32) * scale * gain_ref[:, at]
        ).astype(jnp.bfloat16)
    for level in range(levels):
        for tile in range(TILES):
            for i in range(n_tp >> (level + 1)):
                share(level, tile, i).wait_send()
    for kind in range(2):
        direct(kind, mate).wait_send()

    def sent_on(other, carry):
        for kind in range(2):
            direct(kind, 2 * other + side).wait_send()
        return carry

    lax.fori_loop(pair + 1, n_sp // 2, sent_on, 0)

    def relayed(other, carry):
        for kind in range(2):
            relay(kind, 2 * other + side).wait_send()
        return carry

    lax.fori_loop(0, pair, relayed, 0)


def attention_scratch(n_sp, n_tp, length, kv_width, q_width, width):
    rows = length // n_tp
    levels = n_tp.bit_length() - 1
    kv_local = kv_width // HEAD
    stacked = q_width // kv_width * length
    bf16 = jnp.bfloat16
    dma = pltpu.SemaphoreType.DMA
    return [
        pltpu.VMEM((2, n_sp, length, kv_width), bf16),
        pltpu.VMEM((q_width, width), bf16),
        pltpu.VMEM((kv_local, stacked, HEAD), jnp.float32),
        pltpu.VMEM((kv_local, stacked, 1), jnp.float32),
        tuple(pltpu.VMEM((n_tp >> level, rows, width), bf16) for level in range(levels)),
        tuple(pltpu.VMEM((n_tp >> (level + 1), rows, width), bf16) for level in range(levels)),
        dma,
        dma((2, n_sp)),
        dma((2, n_sp)),
        dma((2, n_sp)),
        dma((levels, TILES, n_tp // 2)),
        dma((levels, TILES, n_tp // 2)),
    ]


def attend(queries, keys, values, break_bias, w_out, residual, ffn_gain):
    n_sp, n_tp = lax.axis_size("sp"), lax.axis_size("tp")
    vmem = pl.BlockSpec(memory_space=pltpu.VMEM)
    shape = jax.ShapeDtypeStruct(residual.shape, jnp.bfloat16)
    return pl.pallas_call(
        functools.partial(attention_part, n_sp, n_tp),
        out_shape=(shape, shape),
        in_specs=[
            vmem, vmem, vmem, pl.BlockSpec(memory_space=pltpu.SMEM),
            pl.BlockSpec(memory_space=pl.ANY), vmem, vmem,
        ],
        out_specs=(vmem, vmem),
        scratch_shapes=attention_scratch(
            n_sp, n_tp, queries.shape[0], keys.shape[1], queries.shape[1], w_out.shape[1]
        ),
        compiler_params=pltpu.CompilerParams(
            has_side_effects=True, vmem_limit_bytes=48 * 1024 * 1024
        ),
        name="attend",
    )(queries, keys, values, break_bias, w_out, residual, ffn_gain[None])


def on_device(
    queries,
    keys,
    values,
    break_bias,
    residual,
    w_out,
    ffn_gain,
    pick_ids,
    pair_logit,
    w_gate,
    w_up,
    w_down,
    out_gain,
):
    length = queries.shape[0]
    stream, ffn_in = attend(queries, keys, values, break_bias, w_out, residual, ffn_gain)
    stream_float = stream.astype(jnp.float32)
    quarters = lax.axis_size("tp")
    quarter = lax.axis_index("tp")
    slice_rows = length // quarters
    width = w_out.shape[1]
    experts = lax.axis_size("sp")
    capacity = max(2, (3 * slice_rows + experts - 1) // experts)
    routed = lax.dynamic_slice_in_dim(pick_ids, quarter * slice_rows, slice_rows, 0)[None]
    blocks = routed.shape[0]
    entries = ffn_in.reshape(blocks, slice_rows, width)
    flat_ids = routed.reshape(blocks, slice_rows * TOP)
    places = jnp.arange(slice_rows * TOP, dtype=jnp.int32)
    earlier = places[None, :] < places[:, None]
    matches = (flat_ids[:, :, None] == flat_ids[:, None, :]) & earlier[None]
    ranks = jnp.sum(matches.astype(jnp.int32), axis=2)
    targets = (flat_ids * capacity + ranks).reshape(blocks, slice_rows, TOP)
    block_ids = jnp.arange(blocks, dtype=jnp.int32)[:, None]
    outgoing = jnp.zeros((blocks, experts * capacity, width), jnp.bfloat16)
    for pick_index in range(TOP):
        outgoing = outgoing.at[block_ids, targets[:, :, pick_index]].set(entries)
    arrived = lax.all_to_all(outgoing, "sp", split_axis=1, concat_axis=1, tiled=True).reshape(
        -1, width
    )
    piece = lax.all_gather(arrived, "tp", axis=0, tiled=True)
    gated = jax.nn.silu(jnp.dot(piece, w_gate[0], preferred_element_type=jnp.float32))
    hidden = (gated * jnp.dot(piece, w_up[0], preferred_element_type=jnp.float32)).astype(
        jnp.bfloat16
    )
    results = lax.psum_scatter(
        jnp.dot(hidden, w_down[0], preferred_element_type=jnp.float32).astype(jnp.bfloat16),
        "tp",
        scatter_dimension=0,
        tiled=True,
    )
    returned = lax.all_to_all(results, "sp", split_axis=0, concat_axis=0, tiled=True)
    own_targets = targets[0]
    logits = lax.dynamic_slice_in_dim(pair_logit, quarter * slice_rows, slice_rows, 0)
    leading = returned[own_targets[:, 0]].astype(jnp.float32)
    trailing = returned[own_targets[:, 1]].astype(jnp.float32)
    blended = (
        jax.nn.sigmoid(logits)[:, None] * leading + jax.nn.sigmoid(-logits)[:, None] * trailing
    )
    blend_scale = lax.rsqrt(jnp.mean(blended * blended, axis=-1, keepdims=True) + epsilon)
    return (stream_float + blended * blend_scale * out_gain).astype(jnp.bfloat16)


def solution(mesh):
    placed = (
        P("sp", "tp"),
        P("sp", "tp"),
        P("sp", "tp"),
        P("tp"),
        P(("sp", "tp"), None),
        P("tp", None),
        P(),
        P("sp", None),
        P("sp"),
        P("sp", None, "tp"),
        P("sp", None, "tp"),
        P("sp", "tp", None),
        P(),
    )
    return jax.shard_map(
        on_device, mesh=mesh, in_specs=placed, out_specs=P(("sp", "tp"), None), check_vma=False
    )
```

time: 277 us -> 232 us (0.84)
  waiting for transfers between devices: 130 us -> 90.2 us
  starting transfers between devices: 39.8 us -> 5.55 us
  blocking collectives: 25.5 us -> 48.9 us
  Pallas kernels: 0 us -> 22.9 us
  other arithmetic: 24.8 us -> 10.5 us
  matrix products: 23.4 us -> 11.2 us
  local copies, waits for them, and re-layouts: 19.4 us -> 28.3 us
    ppermute x7 -> x0, starting transfers between devices: 34.2 us -> none  [passed_along(): return lax.ppermute(block, axis, route)]
    reduce_scatter x1 -> x0, waiting for transfers between devices: 27.4 us -> none  [on_device(): lax.psum_scatter(jnp.dot(head_out, w_out, preferred_element_type=jnp.floa...]
    all_to_all x1, blocking collectives: 25.5 us -> 48.9 us  [on_device(): lax.all_to_all(outgoing, 'sp', split_axis=1, concat_axis=1, tiled=True)]
    pallas_call x0 -> x1, Pallas kernels: none -> 22.9 us  [attend(): pl.pallas_call(functools.partial(attention_part, n_sp, n_tp), out_shape=(...]
    ppermute x7 -> x0, waiting for transfers between devices: 12.4 us -> none  [passed_along(): return lax.ppermute(block, axis, route)]
    dot_general x17 -> x0, matrix products: 12.2 us -> none  [the longest x8 4.49 us: stick_block(): jnp.einsum('qcgs,scd->qcgd', weights.astype(jnp.bfloat16), value_block, p...]
    another operation x9 -> x0, other arithmetic: 9.22 us -> none  [the longest x8 9.21 us: stick_block(): behind = lax.cumsum(breaks, axis=3, reverse=True) - breaks]
    unnamed x28, local copies, waits for them, and re-layouts: 7.1 us -> 12.7 us
  transfers between devices with their start and end apart: 11 -> 3, of which waited for: 11 -> 3; matrix products, arithmetic and copies ran while one was open for 1% -> 0% of each run, Pallas kernels for 0% -> 0%
where the time goes in v1:
time: 232 us; the launch traced here: 231 us
  waiting for transfers between devices  90.2 us (39%)
  blocking collectives  48.9 us (21%)
  local copies, waits for them, and re-layouts  28.3 us (12%)
  Pallas kernels  22.9 us (10%)
  between operations  13.6 us (6%)
  matrix products  11.2 us (5%)
  other arithmetic  10.5 us (5%)
  starting transfers between devices  5.55 us (2%)
    all_to_all x1, blocking collectives, on_device(): lax.all_to_all(outgoing, 'sp', split_axis=1, concat_axis=1, tiled=True)  48.9 us
    reduce_scatter x1, waiting for transfers between devices, on_device(): lax.psum_scatter(jnp.dot(hidden, w_down[0], preferred_element_type=jnp.fl...  38 us
    all_gather x1, waiting for transfers between devices, on_device(): piece = lax.all_gather(arrived, 'tp', axis=0, tiled=True)  26.7 us
    all_to_all x1, waiting for transfers between devices, on_device(): lax.all_to_all(results, 'sp', split_axis=0, concat_axis=0, tiled=True)  25.5 us
    pallas_call x1, Pallas kernels, attend(): pl.pallas_call(functools.partial(attention_part, n_sp, n_tp), out_shape=(...  22.9 us
    unnamed x28, local copies, waits for them, and re-layouts  12.7 us
    dot_general x1, matrix products, on_device(): jnp.dot(hidden, w_down[0], preferred_element_type=jnp.float32)  7.67 us
    unnamed x1, other arithmetic  6.65 us
  transfers between devices with their start and end apart: 3, of which 3 were waited for; matrix products, arithmetic and copies ran while one was open for 0% of the time, Pallas kernels for 0%

profile of v1, /device:TPU:0, one launch (start us, length us, event | category | flops | bytes accessed | tf_op | source)
XLA Modules:
  0.0 231.1 jit_solution(2845695217681659737)
XLA Ops:
  6.5 0.0 copy-start
  6.5 0.0 all-gather.3.cloned.1.call-start
  6.5 0.9 constant_dynamic-slice_fusion
  7.4 0.1 copy.48
  7.5 0.1 eq.23
  7.6 0.2 convert_reduce_fusion
  7.8 0.1 reduce_sum.21
  7.9 0.1 copy.41
  8.1 0.1 copy.49
  8.2 0.1 copy.51
  8.2 0.1 copy.50
  8.3 0.1 copy.52
  8.4 0.1 select_reduce_fusion.1
  8.5 0.1 select_reduce_fusion
  8.6 0.0 copy-start.1
  8.7 2.2 copy-done.1
  10.8 0.0 copy-start.2
  10.8 0.9 copy-done.2
  11.8 0.0 copy-start.3
  11.8 0.9 copy-done.3
  12.7 0.0 copy-start.4
  12.7 0.8 copy-done.4
  13.5 0.0 copy-start.5
  13.5 0.8 copy-done.5
  14.2 0.0 copy-start.6
  14.2 0.7 copy-done.6
  14.9 0.0 copy-start.7
  14.9 0.7 copy-done.7
  15.6 22.9 %attend.1 = (bf16[32,4096]{1,0:T(8,128)(2,1)S(1)}, bf16[32,4096]{1,0:T(8,128)(2,1)S(1)}) custom-call(bf16[128,512]{1,0:T(8,128)(2,1)S(1)} %copy-done.3, bf16[128,128]{1,0:T(8,128)(2,1)S(1)} %copy-done.4, bf16[128,128]{1,0:T(8,128)(2,1)S(1)} %copy-done.5, f32[4]{0:T(128)S(1)} %copy-done.7, bf16[512,4096]{1,0:T(8,128)(2,1)S(1)} %copy-done.1, ...), custom_call_target="tpu_custom_call" | custom-call | tf_op jit(solution)/shard_map/attend/pallas_call | solution.py:237
  38.5 1.2 scatter_custom_fusion
  39.8 1.4 scatter_fusion
  41.2 2.9 %copy.54 = bf16[1,96,4096]{2,0,1:T(2,128)(2,1)} copy(bf16[1,96,4096]{2,1,0:T(8,128)(2,1)S(1)} %bitcast.40) | data formatting | bytes 1572864 | tf_op jit(solution)/shard_map/scatter | solution.py:291
  44.1 0.5 broadcast.139
  44.6 6.7 %reduce.9 = bf16[96,4096]{1,0:T(8,128)(2,1)S(1)} reduce(bf16[96,1,4096]{2,1,0:T(2,128)(2,1)} %bitcast.41, bf16[]{:T(256)} %broadcast.139), dimensions={1}, to_apply=%bitcast.36.reduce_sub_computation | reduce | bytes 1572866
  51.3 1.6 reshape.190
  52.9 48.9 %all_to_all.17 = bf16[8,2,24576]{2,1,0:T(2,128)(2,1)S(1)} all-to-all(bf16[8,2,24576]{2,1,0:T(2,128)(2,1)} %reshape.190), channel_id=1, replica_groups=mesh['sp'=8,'tp'=4] {'sp'}, dimensions={0} | all-to-all | bytes 1572864 | tf_op jit(solution)/shard_map/all_to_all | solution.py:292
  101.8 3.2 %reshape.191 = bf16[96,1,4096]{2,1,0:T(2,128)(2,1)} reshape(bf16[8,2,24576]{2,1,0:T(2,128)(2,1)S(1)} %all_to_all.17) | data formatting | bytes 1572864
  105.0 3.1 %copy.47 = bf16[1,96,4096]{2,1,0:T(8,128)(2,1)} copy(bf16[1,96,4096]{2,0,1:T(2,128)(2,1)} %bitcast.42) | data formatting | bytes 1572864 | tf_op jit(solution)/shard_map/all_to_all | solution.py:292
  108.1 0.0 all-gather.3.cloned.1.call-update
  108.1 0.0 reduce-scatter.2.cloned.1.call-start
  108.2 26.7 %all-gather.3.cloned.1.call-done = bf16[1,384,4096]{2,1,0:T(8,128)(2,1)} async-done(((bf16[1,96,4096]{2,1,0:T(8,128)(2,1)}), bf16[1,384,4096]{2,1,0:T(8,128)(2,1)}) %all-gather.3.cloned.1.call-update) | async-done | bytes 3145744 | tf_op jit(solution)/shard_map/all_gather | solution.py:295
  134.9 3.5 %fusion.2 = f32[384,256]{1,0:T(8,128)S(1)} fusion(bf16[1,384,4096]{2,1,0:T(8,128)(2,1)} %all-gather.3.cloned.1.call-done, bf16[1,4096,256]{2,1,0:T(8,128)(2,1)} %param.22), kind=kOutput, calls=%fused_computation.7 | convolution fusion | flops 805306368 | bytes 5636096 | tf_op jit(solution)/shard_map/dot_general | solution.py:296
  138.4 0.0 copy-done
  138.4 7.7 %convolution_convert_fusion = bf16[384,4096]{1,0:T(8,128)(2,1)} fusion(bf16[1,256,4096]{2,1,0:T(8,128)(2,1)S(1)} %copy-done, bf16[1,4096,256]{2,1,0:T(8,128)(2,1)} %param.23, bf16[1,384,4096]{2,1,0:T(8,128)(2,1)} %all-gather.3.cloned.1.call-done, f32[384,256]{1,0:T(8,128)S(1)} %fusion.2), kind=kOutput, calls=%fused_computation.4 | convolution fusion | flops 1612775424 | bytes 10878976 | tf_op jit(solution)/shard_map/dot_general | solution.py:301
  146.1 0.0 reduce-scatter.2.cloned.1.call-update
  146.1 0.0 copy-start.9
  146.1 38.0 %reduce-scatter.2.cloned.1.call-done = bf16[96,4096]{1,0:T(8,128)(2,1)} async-done(((bf16[384,4096]{1,0:T(8,128)(2,1)}), bf16[96,4096]{1,0:T(8,128)(2,1)}) %reduce-scatter.2.cloned.1.call-update) | async-done | bytes 786448 | tf_op jit(solution)/shard_map/reduce_scatter | solution.py:300
  184.1 2.2 all_to_all.12
  186.3 5.5 %all-to-all-start.1 = ((bf16[8,12,4096]{2,1,0:T(8,128)(2,1)}), bf16[8,12,4096]{2,1,0:T(8,128)(2,1)}, u32[]{:S(2)}, u32[]{:S(2)}) async-start(bf16[8,12,4096]{2,1,0:T(8,128)(2,1)} %all_to_all.12), calls=%async_computation.2 | async-start | bytes 2097152 | tf_op jit(solution)/shard_map/all_to_all | solution.py:306
  191.9 0.0 copy-done.9
  191.9 0.1 add_divide_fusion.1
  191.9 0.2 fusion.30
  192.1 25.5 %all-to-all-done.1 = bf16[8,12,4096]{2,1,0:T(8,128)(2,1)} async-done(((bf16[8,12,4096]{2,1,0:T(8,128)(2,1)}), bf16[8,12,4096]{2,1,0:T(8,128)(2,1)}, u32[]{:S(2)}, u32[]{:S(2)}) %all-to-all-start.1) | async-done | bytes 786464 | tf_op jit(solution)/shard_map/all_to_all | solution.py:306
  217.6 1.4 all_to_all.14
  219.0 0.0 copy-start.8
  219.0 0.7 gather_fusion.1
  219.7 1.4 gather_fusion
  221.1 1.2 multiply_reduce_fusion
  222.4 0.0 copy-done.8
  222.4 1.9 add_convert_fusion
  (7 shorter events, 0.0 us)
Async XLA Ops:
  6.5 131.9 %copy-start = (bf16[1,256,4096]{2,1,0:T(8,128)(2,1)S(1)}, bf16[1,256,4096]{2,1,0:T(8,128)(2,1)}, u32[]{:S(2)}) copy-start(bf16[1,256,4096]{2,1,0:T(8,128)(2,1)} %param.24) | copy-start | bytes 6291460
  6.5 128.3 %all-gather.3.cloned.1.call-start = ((), (), s32[]{:S(2)}) async-start(), calls=%async_computation.4 | async-start | bytes 3932160 | tf_op jit(solution)/shard_map/all_gather | solution.py:295
  8.6 2.2 copy-start.1
  10.8 0.9 copy-start.2
  11.8 0.9 copy-start.3
  12.7 0.8 copy-start.4
  13.5 0.8 copy-start.5
  14.2 0.7 copy-start.6
  14.9 0.7 copy-start.7
  108.1 76.0 %reduce-scatter.2.cloned.1.call-start = ((), (), s32[]{:S(2)}) async-start(), calls=%async_computation.3 | async-start | bytes 3932160 | tf_op jit(solution)/shard_map/reduce_scatter | solution.py:300
  146.1 45.8 %copy-start.9 = (f32[128]{0:T(128)S(1)}, f32[128]{0:T(128)}, u32[]{:S(2)}) copy-start(f32[128]{0:T(128)} %param.21) | copy-start | bytes 1540
  186.3 31.3 %all-to-all-start.1 = ((bf16[8,12,4096]{2,1,0:T(8,128)(2,1)}), bf16[8,12,4096]{2,1,0:T(8,128)(2,1)}, u32[]{:S(2)}, u32[]{:S(2)}) async-start(bf16[8,12,4096]{2,1,0:T(8,128)(2,1)} %all_to_all.12), calls=%async_computation.2 | async-start | bytes 2097152 | tf_op jit(solution)/shard_map/all_to_all | solution.py:306
  219.0 3.4 %copy-start.8 = (f32[4096]{0:T(1024)S(1)}, f32[4096]{0:T(1024)}, u32[]{:S(2)}) copy-start(f32[4096]{0:T(1024)} %param.25) | copy-start | bytes 49156
Sparse Core Ops, SparseCore 0:
  108.2 26.5 all-gather.2
  146.2 37.8 reduce-scatter.1

commit v2 on v1

--- a/solution.py
+++ b/solution.py
@@ -11,6 +11,7 @@
 TOP = 2
 MESH = pl.DeviceIdType.MESH
 TILES = 4
+GROUPS = 4
 
 epsilon = 1e-06
 
@@ -252,6 +253,252 @@
     )(queries, keys, values, break_bias, w_out, residual, ffn_gain[None])
 
 
+def expert_part(
+    capacity, place_ref, back_ref, weight_ref, ffn_ref, stream_ref, gain_ref, gate_ref, up_ref, down_ref,
+    out_ref, gate_buf, up_buf, down_buf, own, packed, landed, slabs, outs, first, total,
+    corner, direct, giving, leaving, given, staged, blend, load_sem, send_sem, recv_sem,
+):
+    me, mine = lax.axis_index("sp"), lax.axis_index("tp")
+    group, member = me // TOP, me % TOP
+    across, core = mine // 2, mine % 2
+    groups = packed.shape[0]
+    half = blend.shape[2]
+    rows = ffn_ref.shape[0]
+    wide = packed.shape[2]
+    cuts = (slice(0, half // 2), slice(half // 2, wide))
+    thin = (slice(0, half // 2), slice(half // 2, half))
+    x_side = (me + 1 - 2 * member, mine)
+    y_side = (me, mine + 2 - 4 * across)
+    twin = (me, mine + 1 - 2 * core)
+    sent = []
+
+    def send(src, dst, device):
+        copy = pltpu.make_async_remote_copy(
+            src_ref=src, dst_ref=dst, send_sem=send_sem.at[len(sent)],
+            recv_sem=recv_sem.at[len(sent)], device_id=device, device_id_type=MESH,
+        )
+        copy.start()
+        sent.append(copy)
+        return copy
+
+    def columns(side):
+        return pl.ds(pl.multiple_of(side * half, half), half)
+
+    swap = send(ffn_ref.at[:, columns(1 - core)], own.at[core], twin)
+    loads = []
+    for at, (src, dst) in enumerate(((gate_ref, gate_buf), (up_ref, up_buf), (down_ref, down_buf))):
+        loads.append(pltpu.make_async_copy(src, dst, load_sem.at[at]))
+        loads[-1].start()
+    kept = ffn_ref[:, columns(core)]
+    place = place_ref[...]
+    slots = packed.shape[1]
+    tail = jnp.dot(place, weight_ref[...], preferred_element_type=jnp.float32)
+    for g in range(groups):
+        packed[g, :, half:] = tail[g * slots : (g + 1) * slots].astype(jnp.bfloat16)
+    swap.wait_recv()
+    other = own[1 - core]
+    lead = jnp.where(core == 0, kept, other)
+    rest = jnp.where(core == 0, other, kept)
+    joined = jnp.concatenate([lead, rest], axis=0)
+    moved = []
+    for cut, body in zip(cuts, thin):
+        rows_out = jnp.dot(place, joined[:, body], preferred_element_type=jnp.float32)
+        for g in range(groups):
+            packed[g, :, body] = rows_out[g * slots : (g + 1) * slots].astype(jnp.bfloat16)
+        step = []
+        for hop in range(1, groups):
+            target = (group + hop) % groups
+            step.append(
+                send(packed.at[target, :, cut], landed.at[group, :, cut], (target * TOP + member, mine))
+            )
+        moved.append(step)
+        landed[group, :, cut] = packed[group, :, cut]
+    beside_x, beside_y, far, shared = [], [], [], []
+    for cut, step in zip(cuts, moved):
+        for copy in step:
+            copy.wait_recv()
+        whole = jnp.concatenate(
+            [landed[g, :, cut].astype(jnp.float32) for g in range(groups)], axis=0
+        )
+        slabs[core, member, across, :, cut] = whole.astype(jnp.bfloat16)
+        here = slabs.at[core, member, across, :, cut]
+        beside_x.append(send(here, here, x_side))
+        beside_y.append(send(here, here, y_side))
+        shared.append(send(here, here, twin))
+    for at, cut in enumerate(cuts):
+        from_y = slabs.at[core, member, 1 - across, :, cut]
+        from_x = slabs.at[core, 1 - member, across, :, cut]
+        beside_y[at].wait_recv()
+        if at == 0:
+            far.append(send(from_y, from_y, x_side))
+        shared.append(send(from_y, from_y, twin))
+        beside_x[at].wait_recv()
+        if at == 1:
+            far.append(send(from_x, from_x, y_side))
+    for at, cut in enumerate(cuts):
+        from_x = slabs.at[core, 1 - member, across, :, cut]
+        shared.append(send(from_x, from_x, twin))
+    for copy in loads:
+        copy.wait()
+
+    def run(which):
+        lefts = [slabs[side, which].reshape(-1, wide) for side in range(2)]
+        gate, up = (
+            sum(
+                jnp.dot(
+                    lefts[side][:, :half], buf[side * half : (side + 1) * half],
+                    preferred_element_type=jnp.float32,
+                )
+                for side in range(2)
+            )
+            for buf in (gate_buf, up_buf)
+        )
+        hidden = (gate / (1.0 + jnp.exp(-gate)) * up).astype(jnp.bfloat16)
+        shares = lefts[0][:, half : half + HEAD].astype(jnp.float32)
+        share = jnp.where(
+            member == 0, shares[:, 0:1] + shares[:, 1:2], shares[:, 2:3] + shares[:, 3:4]
+        )
+        for side in range(2):
+            for body in thin:
+                at = slice(side * half + body.start, side * half + body.stop)
+                result = jnp.dot(hidden, down_buf[:, at], preferred_element_type=jnp.float32)
+                result = (result * share).astype(jnp.bfloat16)
+                outs[side, which, :, :, body] = result.reshape(2, -1, half // 2)
+
+    for copy in shared[:4]:
+        copy.wait_recv()
+    run(member)
+    for at, cut in enumerate(cuts):
+        far[at].wait_recv()
+        diagonal = slabs.at[core, 1 - member, 1 - across, :, cut]
+        shared.append(send(diagonal, diagonal, twin))
+    sums = []
+    sums.append([
+        send(outs.at[1 - core, member, :, :, body], first.at[member, :, :, body], twin)
+        for body in thin
+    ])
+    for copy in shared[4:]:
+        copy.wait_recv()
+    run(1 - member)
+    sums.append([
+        send(outs.at[1 - core, 1 - member, :, :, body], first.at[1 - member, :, :, body], twin)
+        for body in thin
+    ])
+    real = jnp.float32
+    for copies, which in zip(sums, (member, 1 - member)):
+        for copy, body in zip(copies, thin):
+            copy.wait_recv()
+            added = outs[core, which, :, :, body].astype(real) + first[which, :, :, body].astype(real)
+            total[which, :, :, body] = added.astype(jnp.bfloat16)
+    diagonal = total.at[1 - member, 1 - across]
+    to_y = send(diagonal.at[:, thin[0]], corner.at[0], y_side)
+    to_x = send(diagonal.at[:, thin[1]], corner.at[1], x_side)
+    x_slab = total.at[1 - member, across]
+    y_slab = total.at[member, 1 - across]
+    got = [[None, None], [None, None]]
+    got[0][1] = send(x_slab.at[:, thin[1]], direct.at[0, :, thin[1]], x_side)
+    got[1][0] = send(y_slab.at[:, thin[0]], direct.at[1, :, thin[0]], y_side)
+    to_y.wait_recv()
+    giving[0] = (total[1 - member, across, :, thin[0]].astype(real) + corner[0].astype(real)).astype(jnp.bfloat16)
+    got[0][0] = send(giving.at[0], direct.at[0, :, thin[0]], x_side)
+    to_x.wait_recv()
+    giving[1] = (total[member, 1 - across, :, thin[1]].astype(real) + corner[1].astype(real)).astype(jnp.bfloat16)
+    got[1][1] = send(giving.at[1], direct.at[1, :, thin[1]], y_side)
+    for at, body in enumerate(thin):
+        got[0][at].wait_recv()
+        got[1][at].wait_recv()
+        final = (
+            total[member, across, :, body].astype(real)
+            + direct[0, :, body].astype(real)
+            + direct[1, :, body].astype(real)
+        )
+        for g in range(groups):
+            leaving[g, :, body] = final[g * slots : (g + 1) * slots].astype(jnp.bfloat16)
+    returns = []
+    for body in thin:
+        step = []
+        for hop in range(1, groups):
+            target = (group + hop) % groups
+            step.append(
+                send(leaving.at[target, :, body], given.at[group, :, body], (target * TOP + member, mine))
+            )
+        returns.append(step)
+        given[group, :, body] = leaving[group, :, body]
+    for body, step in zip(thin, returns):
+        for copy in step:
+            copy.wait_recv()
+        whole = jnp.concatenate([given[g, :, body].astype(real) for g in range(groups)], axis=0)
+        back = jnp.dot(back_ref[...], whole.astype(jnp.bfloat16), preferred_element_type=real)
+        staged[:, :, body] = back.astype(jnp.bfloat16).reshape(2, rows, half // 2)
+    last = send(staged.at[1 - core], blend.at[core], twin)
+    squares = jnp.sum(staged[core].astype(real) ** 2, axis=1, keepdims=True)
+    last.wait_recv()
+    squares += jnp.sum(blend[1 - core].astype(real) ** 2, axis=1, keepdims=True)
+    scale = lax.rsqrt(squares / (2 * half) + epsilon)
+    for side, source in ((core, staged), (1 - core, blend)):
+        at = columns(side)
+        out_ref[:, at] = (
+            stream_ref[:, at].astype(real) + source[side].astype(real) * scale * gain_ref[:, at]
+        ).astype(jnp.bfloat16)
+    for copy in sent:
+        copy.wait_send()
+
+
+def grouped_experts(capacity, ffn_in, stream, pick_ids, pair_logit, w_gate, w_up, w_down, out_gain):
+    rows, width = stream.shape
+    groups = lax.axis_size("sp") // TOP
+    across = lax.axis_index("tp") // 2
+    chip_rows, slots, half = 2 * rows, 2 * capacity, width // 2
+    picks = lax.dynamic_slice_in_dim(pick_ids, across * chip_rows, chip_rows, 0)
+    logits = lax.dynamic_slice_in_dim(pair_logit, across * chip_rows, chip_rows, 0)
+    chosen = picks[:, 0] // TOP
+    at = jnp.arange(chip_rows, dtype=jnp.int32)
+    same = (chosen[None, :] == chosen[:, None]) & (at[None, :] < at[:, None])
+    target = chosen * slots + jnp.sum(same.astype(jnp.int32), axis=1)
+    place = (target[None, :] == jnp.arange(groups * slots, dtype=jnp.int32)[:, None]).astype(jnp.bfloat16)
+    sign = jnp.where(picks[:, 0] % TOP == 0, 1.0, -1.0)
+    shares = jnp.stack([jax.nn.sigmoid(sign * logits), jax.nn.sigmoid(-sign * logits)], axis=1)
+    coarse = lax.reduce_precision(shares, 8, 7)
+    parts = jnp.stack([coarse, shares - coarse], axis=2).reshape(chip_rows, 2 * TOP)
+    parts = jnp.pad(parts.astype(jnp.bfloat16), ((0, 0), (0, HEAD - 2 * TOP)))
+    vmem = pl.BlockSpec(memory_space=pltpu.VMEM)
+    hbm = pl.BlockSpec(memory_space=pl.ANY)
+    block = groups * slots
+
+    def room(*shape):
+        return pltpu.VMEM(shape, jnp.bfloat16)
+
+    dma = pltpu.SemaphoreType.DMA
+    return pl.pallas_call(
+        functools.partial(expert_part, capacity),
+        out_shape=jax.ShapeDtypeStruct(stream.shape, jnp.bfloat16),
+        in_specs=[vmem] * 6 + [hbm] * 3,
+        out_specs=vmem,
+        scratch_shapes=[
+            room(*w_gate.shape), room(*w_up.shape), room(*w_down.shape),
+            room(2, rows, half),
+            room(groups, slots, half + HEAD),
+            room(groups, slots, half + HEAD),
+            room(2, TOP, 2, block, half + HEAD),
+            room(2, TOP, 2, block, half),
+            room(TOP, 2, block, half),
+            room(TOP, 2, block, half),
+            room(2, block, half // 2),
+            room(2, block, half),
+            room(2, block, half // 2),
+            room(groups, slots, half),
+            room(groups, slots, half),
+            room(2, rows, half),
+            room(2, rows, half),
+            dma((3,)), dma((64,)), dma((64,)),
+        ],
+        compiler_params=pltpu.CompilerParams(
+            has_side_effects=True, vmem_limit_bytes=56 * 1024 * 1024
+        ),
+        name="experts",
+    )(place, place.T, parts, ffn_in, stream, out_gain[None], w_gate, w_up, w_down)
+
+
 def on_device(
     queries,
     keys,
@@ -276,6 +523,10 @@
     width = w_out.shape[1]
     experts = lax.axis_size("sp")
     capacity = max(2, (3 * slice_rows + experts - 1) // experts)
+    if experts == GROUPS * TOP and quarters == 4:
+        return grouped_experts(
+            capacity, ffn_in, stream, pick_ids, pair_logit, w_gate[0], w_up[0], w_down[0], out_gain
+        )
     routed = lax.dynamic_slice_in_dim(pick_ids, quarter * slice_rows, slice_rows, 0)[None]
     blocks = routed.shape[0]
     entries = ffn_in.reshape(blocks, slice_rows, width)

time: 232 us -> 122 us (0.53)
  waiting for transfers between devices: 90.2 us -> 0 us
  Pallas kernels: 22.9 us -> 107 us
  blocking collectives: 48.9 us -> 0 us
  local copies, waits for them, and re-layouts: 28.3 us -> 11.5 us
  between operations: 13.6 us -> 0.06 us
  matrix products: 11.2 us -> 0 us
  other arithmetic: 10.5 us -> 2.98 us
  starting transfers between devices: 5.55 us -> 0 us
    pallas_call x0 -> x1, Pallas kernels: none -> 84.2 us  [grouped_experts(): pl.pallas_call(functools.partial(expert_part, capacity), out_shape=jax.Sh...]
    all_to_all x1 -> x0, blocking collectives: 48.9 us -> none  [on_device(): lax.all_to_all(outgoing, 'sp', split_axis=1, concat_axis=1, tiled=True)]
    reduce_scatter x1 -> x0, waiting for transfers between devices: 38 us -> none  [on_device(): lax.psum_scatter(jnp.dot(hidden, w_down[0], preferred_element_type=jnp.fl...]
    all_gather x1 -> x0, waiting for transfers between devices: 26.7 us -> none  [on_device(): piece = lax.all_gather(arrived, 'tp', axis=0, tiled=True)]
    all_to_all x1 -> x0, waiting for transfers between devices: 25.5 us -> none  [on_device(): lax.all_to_all(results, 'sp', split_axis=0, concat_axis=0, tiled=True)]
    dot_general x2 -> x0, matrix products: 11.2 us -> none  [the longest x1 7.67 us: on_device(): jnp.dot(hidden, w_down[0], preferred_element_type=jnp.float32)]
    all_to_all x3 -> x0, local copies, waits for them, and re-layouts: 6.7 us -> none  [the longest x2 3.56 us: on_device(): lax.all_to_all(results, 'sp', split_axis=0, concat_axis=0, tiled=True)]
    unnamed x1 -> x0, other arithmetic: 6.65 us -> none
  transfers between devices with their start and end apart: 3 -> 0, of which waited for: 3 -> 0; matrix products, arithmetic and copies ran while one was open for 0% -> 0% of each run, Pallas kernels for 0% -> 0%
where the time goes in v2:
time: 122 us
  Pallas kernels  107 us (88%)
  local copies, waits for them, and re-layouts  11.5 us (9%)
  other arithmetic  2.98 us (2%)
    pallas_call x1, Pallas kernels, grouped_experts(): pl.pallas_call(functools.partial(expert_part, capacity), out_shape=jax.Sh...  84.2 us
    pallas_call x1, Pallas kernels, attend(): pl.pallas_call(functools.partial(attention_part, n_sp, n_tp), out_shape=(...  22.9 us
    unnamed x21, local copies, waits for them, and re-layouts  10.7 us

profile of v2, /device:TPU:0, one launch (start us, length us, event | category | flops | bytes accessed | tf_op | source)
XLA Modules:
  0.0 121.6 jit_solution(14602843048912488992)
XLA Ops:
  0.0 0.0 copy-start
  0.0 0.7 copy-done
  0.7 0.1 constant_dynamic-slice_fusion
  0.8 0.7 divide_bitcast_fusion.1
  1.5 0.2 convert_reduce_fusion
  1.7 0.7 divide_bitcast_fusion
  2.5 0.1 copy.16
  2.6 0.6 pad.4.weight_ref
  3.2 0.7 fusion.2.back_ref
  3.9 0.6 fusion.place_ref
  4.5 0.0 copy-start.1
  4.5 2.2 %copy-done.1 = bf16[512,4096]{1,0:T(8,128)(2,1)S(1)} copy-done((bf16[512,4096]{1,0:T(8,128)(2,1)S(1)}, bf16[512,4096]{1,0:T(8,128)(2,1)}, u32[]{:S(2)}) %copy-start.1) | copy-done | bytes 4194328
  6.7 0.0 copy-start.2
  6.7 0.9 copy-done.2
  7.6 0.0 copy-start.5
  7.6 0.9 copy-done.5
  8.5 0.0 copy-start.6
  8.5 0.8 copy-done.6
  9.3 0.0 copy-start.7
  9.3 0.8 copy-done.7
  10.1 0.0 copy-start.8
  10.1 0.7 copy-done.8
  10.8 0.0 copy-start.9
  10.8 0.7 copy-done.9
  11.4 22.9 %attend.1 = (bf16[32,4096]{1,0:T(8,128)(2,1)S(1)}, bf16[32,4096]{1,0:T(8,128)(2,1)S(1)}) custom-call(bf16[128,512]{1,0:T(8,128)(2,1)S(1)} %copy-done.5, bf16[128,128]{1,0:T(8,128)(2,1)S(1)} %copy-done.6, bf16[128,128]{1,0:T(8,128)(2,1)S(1)} %copy-done.7, f32[4]{0:T(128)S(1)} %copy-done.9, bf16[512,4096]{1,0:T(8,128)(2,1)S(1)} %copy-done.1, ...), custom_call_target="tpu_custom_call" | custom-call | tf_op jit(solution)/shard_map/attend/pallas_call | solution.py:238
  34.4 0.0 copy-start.3
  34.4 0.7 copy-done.3
  35.1 0.0 copy-start.4
  35.1 0.7 copy-done.4
  35.8 84.2 %experts.1 = bf16[32,4096]{1,0:T(8,128)(2,1)} custom-call(bf16[96,64]{1,0:T(8,128)(2,1)} %fusion.place_ref, bf16[64,96]{1,0:T(8,128)(2,1)} %fusion.2.back_ref, bf16[64,128]{1,0:T(8,128)(2,1)} %pad.4.weight_ref, bf16[32,4096]{1,0:T(8,128)(2,1)} %copy-done.4, bf16[32,4096]{1,0:T(8,128)(2,1)} %copy-done.3, f32[1,4096]{1,0:T(1,128)} %bitcast.28, ...), custom_call_target="tpu_custom_call" | custom-call | tf_op jit(solution)/shard_map/experts/pallas_call | solution.py:472
  120.0 1.7 %copy.18 = bf16[32,4096]{1,0:T(8,128)(2,1)} copy(bf16[32,4096]{1,0:T(8,128)(2,1)} %experts.1) | data formatting | bytes 524288
  (5 shorter events, 0.0 us)
Async XLA Ops:
  0.0 0.7 copy-start
  4.5 2.2 %copy-start.1 = (bf16[512,4096]{1,0:T(8,128)(2,1)S(1)}, bf16[512,4096]{1,0:T(8,128)(2,1)}, u32[]{:S(2)}) copy-start(bf16[512,4096]{1,0:T(8,128)(2,1)} %w_ref.1) | copy-start | bytes 12582916
  6.7 0.9 copy-start.2
  7.6 0.9 copy-start.5
  8.5 0.8 copy-start.6
  9.3 0.8 copy-start.7
  10.1 0.7 copy-start.8
  10.8 0.7 copy-start.9
  34.4 0.7 copy-start.3
  35.1 0.7 copy-start.4

commit v3 on v2

--- a/solution.py
+++ b/solution.py
@@ -23,7 +23,7 @@
         query, key_block, (((1,), (1,)), ((), ())), preferred_element_type=jnp.float32
     )
     scores = scores * HEAD ** (-0.5) + bias
-    breaks = jnp.maximum(scores, 0.0) + jnp.log1p(jnp.exp(-jnp.abs(scores)))
+    breaks = jnp.maximum(scores, 0.0) + jnp.log(1.0 + jnp.exp(-jnp.abs(scores)))
     stays = scores - breaks
     if diagonal:
         at_row = lax.broadcasted_iota(jnp.int32, (rows, length), 0) % length
@@ -49,8 +49,8 @@
 
 
 def attention_part(
-    n_sp, n_tp, q_ref, k_ref, v_ref, bias_ref, w_ref, res_ref, gain_ref,
-    stream_ref, ffn_ref, kv_buf, w_buf, accs, useds, parts, recvs,
+    n_sp, n_tp, q_hbm, k_hbm, v_hbm, bias_ref, w_ref, res_hbm, gain_hbm,
+    stream_ref, ffn_ref, q_ref, k_ref, v_ref, res_ref, gain_ref, in_sem, kv_buf, w_buf, accs, useds, parts, recvs,
     w_sem, kv_send, kv_relay, kv_recv, rs_send, rs_recv,
 ):
     me, mine = lax.axis_index("sp"), lax.axis_index("tp")
@@ -60,8 +60,18 @@
     rows = length // n_tp
     width = w_buf.shape[1]
     cols = width // TILES
+    arriving = [
+        pltpu.make_async_copy(src, dst, in_sem.at[at])
+        for at, (src, dst) in enumerate((
+            (k_hbm, k_ref), (v_hbm, v_ref), (q_hbm, q_ref), (res_hbm, res_ref), (gain_hbm, gain_ref),
+        ))
+    ]
+    for copy in arriving:
+        copy.start()
     load = pltpu.make_async_copy(w_ref, w_buf, w_sem)
     load.start()
+    for copy in arriving[:2]:
+        copy.wait()
     pair, side = me // 2, me % 2
     mate = me + 1 - 2 * side
     sources = (k_ref, v_ref)
@@ -90,6 +100,7 @@
 
     lax.fori_loop(pair + 1, n_sp // 2, send_on, 0)
 
+    arriving[2].wait()
     queries, biases = [], []
     for c in range(kv_local):
         heads = [c * per_key + g for g in range(per_key)]
@@ -159,6 +170,8 @@
         parts[0][:, :, at] = product.astype(jnp.bfloat16).reshape(n_tp, rows, cols)
         for i in range(n_tp // 2):
             share(0, tile, i).start()
+    for copy in arriving[3:]:
+        copy.wait()
     squares = jnp.zeros((rows, 1), jnp.float32)
     for level in range(levels):
         bit = (mine >> level) % 2
@@ -216,6 +229,12 @@
     bf16 = jnp.bfloat16
     dma = pltpu.SemaphoreType.DMA
     return [
+        pltpu.VMEM((length, q_width), bf16),
+        pltpu.VMEM((length, kv_width), bf16),
+        pltpu.VMEM((length, kv_width), bf16),
+        pltpu.VMEM((rows, width), bf16),
+        pltpu.VMEM((1, width), jnp.float32),
+        dma((5,)),
         pltpu.VMEM((2, n_sp, length, kv_width), bf16),
         pltpu.VMEM((q_width, width), bf16),
         pltpu.VMEM((kv_local, stacked, HEAD), jnp.float32),
@@ -234,27 +253,25 @@
 def attend(queries, keys, values, break_bias, w_out, residual, ffn_gain):
     n_sp, n_tp = lax.axis_size("sp"), lax.axis_size("tp")
     vmem = pl.BlockSpec(memory_space=pltpu.VMEM)
+    hbm = pl.BlockSpec(memory_space=pl.ANY)
     shape = jax.ShapeDtypeStruct(residual.shape, jnp.bfloat16)
     return pl.pallas_call(
         functools.partial(attention_part, n_sp, n_tp),
         out_shape=(shape, shape),
-        in_specs=[
-            vmem, vmem, vmem, pl.BlockSpec(memory_space=pltpu.SMEM),
-            pl.BlockSpec(memory_space=pl.ANY), vmem, vmem,
-        ],
+        in_specs=[hbm, hbm, hbm, pl.BlockSpec(memory_space=pltpu.SMEM), hbm, hbm, hbm],
         out_specs=(vmem, vmem),
         scratch_shapes=attention_scratch(
             n_sp, n_tp, queries.shape[0], keys.shape[1], queries.shape[1], w_out.shape[1]
         ),
         compiler_params=pltpu.CompilerParams(
-            has_side_effects=True, vmem_limit_bytes=48 * 1024 * 1024
+            has_side_effects=True, vmem_limit_bytes=63 * 1024 * 1024
         ),
         name="attend",
     )(queries, keys, values, break_bias, w_out, residual, ffn_gain[None])
 
 
 def expert_part(
-    capacity, place_ref, back_ref, weight_ref, ffn_ref, stream_ref, gain_ref, gate_ref, up_ref, down_ref,
+    place_ref, back_ref, weight_ref, ffn_ref, stream_ref, gain_ref, gate_ref, up_ref, down_ref,
     out_ref, gate_buf, up_buf, down_buf, own, packed, landed, slabs, outs, first, total,
     corner, direct, giving, leaving, given, staged, blend, load_sem, send_sem, recv_sem,
 ):
@@ -404,6 +421,7 @@
     to_x.wait_recv()
     giving[1] = (total[member, 1 - across, :, thin[1]].astype(real) + corner[1].astype(real)).astype(jnp.bfloat16)
     got[1][1] = send(giving.at[1], direct.at[1, :, thin[1]], y_side)
+    returns = []
     for at, body in enumerate(thin):
         got[0][at].wait_recv()
         got[1][at].wait_recv()
@@ -414,8 +432,6 @@
         )
         for g in range(groups):
             leaving[g, :, body] = final[g * slots : (g + 1) * slots].astype(jnp.bfloat16)
-    returns = []
-    for body in thin:
         step = []
         for hop in range(1, groups):
             target = (group + hop) % groups
@@ -444,8 +460,30 @@
         copy.wait_send()
 
 
-def grouped_experts(capacity, ffn_in, stream, pick_ids, pair_logit, w_gate, w_up, w_down, out_gain):
-    rows, width = stream.shape
+def layer_part(
+    n_sp, n_tp, attended, q_hbm, k_hbm, v_hbm, bias_ref, w_ref, res_hbm, gain_hbm,
+    place_ref, back_ref, weight_ref, out_gain_ref, gate_ref, up_ref, down_ref, out_ref,
+    stream_ref, ffn_ref, *scratch,
+):
+    attention_part(
+        n_sp, n_tp, q_hbm, k_hbm, v_hbm, bias_ref, w_ref, res_hbm, gain_hbm,
+        stream_ref, ffn_ref, *scratch[:attended],
+    )
+    expert_part(
+        place_ref, back_ref, weight_ref, ffn_ref, stream_ref, out_gain_ref,
+        gate_ref, up_ref, down_ref, out_ref, *scratch[attended:],
+    )
+
+
+def whole_layer(
+    capacity, queries, keys, values, break_bias, w_out, residual, ffn_gain,
+    pick_ids, pair_logit, w_gate, w_up, w_down, out_gain,
+):
+    n_sp, n_tp = lax.axis_size("sp"), lax.axis_size("tp")
+    rows, width = residual.shape
+    attention = attention_scratch(
+        n_sp, n_tp, queries.shape[0], keys.shape[1], queries.shape[1], w_out.shape[1]
+    )
     groups = lax.axis_size("sp") // TOP
     across = lax.axis_index("tp") // 2
     chip_rows, slots, half = 2 * rows, 2 * capacity, width // 2
@@ -470,11 +508,16 @@
 
     dma = pltpu.SemaphoreType.DMA
     return pl.pallas_call(
-        functools.partial(expert_part, capacity),
-        out_shape=jax.ShapeDtypeStruct(stream.shape, jnp.bfloat16),
-        in_specs=[vmem] * 6 + [hbm] * 3,
+        functools.partial(layer_part, n_sp, n_tp, len(attention)),
+        out_shape=jax.ShapeDtypeStruct(residual.shape, jnp.bfloat16),
+        in_specs=[hbm] * 3
+        + [pl.BlockSpec(memory_space=pltpu.SMEM)]
+        + [hbm] * 3
+        + [vmem] * 4
+        + [hbm] * 3,
         out_specs=vmem,
         scratch_shapes=[
+            room(rows, width), room(rows, width), *attention,
             room(*w_gate.shape), room(*w_up.shape), room(*w_down.shape),
             room(2, rows, half),
             room(groups, slots, half + HEAD),
@@ -493,10 +536,13 @@
             dma((3,)), dma((64,)), dma((64,)),
         ],
         compiler_params=pltpu.CompilerParams(
-            has_side_effects=True, vmem_limit_bytes=56 * 1024 * 1024
+            has_side_effects=True, vmem_limit_bytes=63 * 1024 * 1024
         ),
-        name="experts",
-    )(place, place.T, parts, ffn_in, stream, out_gain[None], w_gate, w_up, w_down)
+        name="layer",
+    )(
+        queries, keys, values, break_bias, w_out, residual, ffn_gain[None],
+        place, place.T, parts, out_gain[None], w_gate, w_up, w_down,
+    )
 
 
 def on_device(
@@ -515,18 +561,19 @@
     out_gain,
 ):
     length = queries.shape[0]
-    stream, ffn_in = attend(queries, keys, values, break_bias, w_out, residual, ffn_gain)
-    stream_float = stream.astype(jnp.float32)
     quarters = lax.axis_size("tp")
     quarter = lax.axis_index("tp")
     slice_rows = length // quarters
     width = w_out.shape[1]
     experts = lax.axis_size("sp")
-    capacity = max(2, (3 * slice_rows + experts - 1) // experts)
+    capacity = max(TOP, (3 * slice_rows + experts - 1) // experts)
     if experts == GROUPS * TOP and quarters == 4:
-        return grouped_experts(
-            capacity, ffn_in, stream, pick_ids, pair_logit, w_gate[0], w_up[0], w_down[0], out_gain
-        )
+        return whole_layer(
+            capacity, queries, keys, values, break_bias, w_out, residual, ffn_gain,
+            pick_ids, pair_logit, w_gate[0], w_up[0], w_down[0], out_gain,
+        )
+    stream, ffn_in = attend(queries, keys, values, break_bias, w_out, residual, ffn_gain)
+    stream_float = stream.astype(jnp.float32)
     routed = lax.dynamic_slice_in_dim(pick_ids, quarter * slice_rows, slice_rows, 0)[None]
     blocks = routed.shape[0]
     entries = ffn_in.reshape(blocks, slice_rows, width)

time: 122 us -> 106 us (0.87)
  local copies, waits for them, and re-layouts: 11.5 us -> 3.15 us
  Pallas kernels: 107 us -> 99.8 us
    unnamed x21 -> x3, local copies, waits for them, and re-layouts: 10.7 us -> 2.35 us
    pallas_call x2 -> x1, Pallas kernels: 107 us -> 99.8 us  [whole_layer(): pl.pallas_call(functools.partial(layer_part, n_sp, n_tp, len(attention)),...]
where the time goes in v3:
time: 106 us
  Pallas kernels  99.8 us (94%)
  local copies, waits for them, and re-layouts  3.15 us (3%)
  other arithmetic  2.99 us (3%)
    pallas_call x1, Pallas kernels, whole_layer(): pl.pallas_call(functools.partial(layer_part, n_sp, n_tp, len(attention)),...  99.8 us
    unnamed x3, local copies, waits for them, and re-layouts  2.35 us

profile of v3, /device:TPU:0, one launch (start us, length us, event | category | flops | bytes accessed | tf_op | source)
XLA Modules:
  0.0 106.0 jit_solution(16735849249997407024)
XLA Ops:
  0.0 0.0 copy-start
  0.0 0.7 copy-done
  0.7 0.1 constant_dynamic-slice_fusion
  0.8 0.7 divide_bitcast_fusion.1
  1.5 0.2 convert_reduce_fusion
  1.7 0.7 divide_bitcast_fusion
  2.5 0.1 copy.16
  2.6 0.6 pad.4.weight_ref
  3.2 0.7 fusion.2.back_ref
  3.9 0.6 fusion.place_ref
  4.5 99.8 %layer.1 = bf16[32,4096]{1,0:T(8,128)(2,1)} custom-call(bf16[128,512]{1,0:T(8,128)(2,1)} %q_hbm.1, bf16[128,128]{1,0:T(8,128)(2,1)} %k_hbm.1, bf16[128,128]{1,0:T(8,128)(2,1)} %v_hbm.1, f32[4]{0:T(128)} %bias_ref.1, bf16[512,4096]{1,0:T(8,128)(2,1)} %w_ref.1, bf16[32,4096]{1,0:T(8,128)(2,1)} %res_hbm.1, f32[1,4096]{1,0:T(1,128)} %bitcast.27, ...), custom_call_target="tpu_custom_call" | custom-call | tf_op jit(solution)/shard_map/layer/pallas_call | solution.py:510
  104.4 1.7 %copy.18 = bf16[32,4096]{1,0:T(8,128)(2,1)} copy(bf16[32,4096]{1,0:T(8,128)(2,1)} %layer.1) | data formatting | bytes 524288
  (5 shorter events, 0.0 us)
Async XLA Ops:
  0.0 0.7 copy-start
